TPU v7x, 32 devices: a whole 2x2x4 slice. The times are simulated.
32 devices in a mesh: sp: 8 (over z, x), tp: 4 (over y, core).
Axes of the slice: x: 2, y: 2, z: 4, core: 2. Of those that a mesh axis runs over, the one named last changes fastest.
Arguments:
- conv_value: bfloat16 [4096, 1024], P('sp', 'tp'), may hold values from -6 to 6
- conv_gate: bfloat16 [4096, 1024], P('sp', 'tp'), may hold values from -9 to 9
- conv_weight: float32 [31, 1024], P(None, 'tp'), may hold values from -2.2 to 2.2
- conv_gain: float32 [1024], P('tp'), may hold values from 0.1 to 1.9
- conv_shift: float32 [1024], P('tp'), may hold values from -3 to 3
- out_weight: bfloat16 [1024, 2048], P('tp'), may hold values from -0.1875 to 0.1875
- residual: bfloat16 [4096, 2048], P('sp', 'tp'), may hold values from -10 to 10
- mix_gain: float32 [2048], P('tp'), may hold values from 0.1 to 1.9
- expert_ids: int32 [4096, 2], P('sp'), may hold values from 0 to 7, all different within a row; in each aligned block of 128 rows (0 to 127, 128 to 255, ...) at most 64 rows name the same one
- group_weight: float32 [4096], P('sp'), may hold values from 0.6 to 1
- score_gap: float32 [4096], P('sp'), may hold values from -0.8 to 0.8
- w_gate: bfloat16 [8, 2048, 1024], P('sp', None, 'tp'), may hold values from -0.125 to 0.125
- w_up: bfloat16 [8, 2048, 1024], P('sp', None, 'tp'), may hold values from -0.125 to 0.125
- w_down: bfloat16 [8, 1024, 2048], P('sp', 'tp'), may hold values from -0.1875 to 0.1875
Outputs:
- layer_out: bfloat16 [4096, 2048], P('sp', 'tp')
Inputs may be any that keep to these rules, and one draw needn't show every extreme that they name: `expert_ids`: the two experts of a position differ. In each aligned block of 512 // 4 positions no expert is named by more than 64 rows, a bound that some block reaches.
All inputs are finite; a program needn't handle non-finite values.
Results may differ from a plain program's by a relative error of at most 0.012.
Values may be sent and summed in bfloat16 or wider, within the bound.
No kernel may reach another device: no remote copies, remote signals or barrier semaphores. Data moves between devices by JAX's collectives and lax.ppermute only.
A program may use at most 128 MiB of HBM per device.

v0:
```python
import jax
import jax.numpy as jnp
from jax import lax
from jax.sharding import PartitionSpec as P

D = 2048
CH = 1024
eps = 1e-06


def passed_along(value, axis, steps):
    count = lax.axis_size(axis)
    leading, last = (max(0, -steps), min(count, count - steps))
    return lax.ppermute(value, axis, [(source, source + steps) for source in range(leading, last)])


def shards(
    conv_value,
    conv_gate,
    conv_weight,
    conv_gain,
    conv_shift,
    out_weight,
    residual,
    mix_gain,
    expert_ids,
    group_weight,
    score_gap,
    w_gate,
    w_up,
    w_down,
):
    row_count = conv_value.shape[0]
    reach_rows = conv_weight.shape[0] - 1
    seq_devices = lax.axis_size("sp")
    tp_devices = lax.axis_size("tp")
    prev_value, prev_gate = passed_along(
        (conv_value[row_count - reach_rows :], conv_gate[row_count - reach_rows :]), "sp", 1
    )
    values = jnp.concatenate([prev_value, conv_value], axis=0).astype(jnp.float32)
    gate_pre = jnp.concatenate([prev_gate, conv_gate], axis=0).astype(jnp.float32)
    gated = values * jax.nn.sigmoid(gate_pre)
    convolved = jnp.zeros((row_count, conv_value.shape[1]), jnp.float32)
    for tap_index in range(reach_rows + 1):
        convolved = convolved + conv_weight[tap_index] * gated[tap_index : tap_index + row_count]
    row_sum, squares = lax.psum(
        (jnp.sum(convolved, axis=-1), jnp.sum(convolved * convolved, axis=-1)), "tp"
    )
    row_mean = (row_sum / CH)[:, None]
    row_var = (squares / CH)[:, None] - row_mean * row_mean
    normalized = (convolved - row_mean) * lax.rsqrt(row_var + eps) * conv_gain + conv_shift
    activated = jax.nn.silu(normalized).astype(jnp.bfloat16)
    partial_out = jnp.dot(activated, out_weight, preferred_element_type=jnp.float32)
    mixed = lax.psum_scatter(
        partial_out.astype(jnp.bfloat16), "tp", scatter_dimension=1, tiled=True
    ).astype(jnp.float32)
    middle = (residual.astype(jnp.float32) + mixed).astype(jnp.bfloat16)
    middle_wide = middle.astype(jnp.float32)
    row_sq = lax.psum(jnp.sum(middle_wide * middle_wide, axis=-1), "tp")
    normed = (middle_wide * lax.rsqrt(row_sq / D + eps)[:, None] * mix_gain).astype(jnp.bfloat16)
    quarter = row_count // tp_devices
    capacity = 4 * quarter // seq_devices
    expert_num = expert_ids.reshape(tp_devices, quarter * 2)
    onehot = (
        expert_num[:, :, None] == jnp.arange(seq_devices, dtype=jnp.int32)[None, None, :]
    ).astype(jnp.int32)
    before = jnp.cumsum(onehot, axis=1) - onehot
    ranking = jnp.sum(before * onehot, axis=-1)
    quarter_index = jnp.arange(tp_devices, dtype=jnp.int32)[:, None]
    slots = ((expert_num * tp_devices + quarter_index) * capacity + ranking).reshape(-1)
    own_rows = lax.all_to_all(normed, "tp", split_axis=0, concat_axis=1, tiled=True)
    my_index = lax.axis_index("tp")
    own_experts = lax.dynamic_slice_in_dim(expert_num, my_index, 1, 0)[0]
    own_rank = lax.dynamic_slice_in_dim(ranking, my_index, 1, 0)[0]
    own_slots = own_experts * capacity + own_rank
    token_of = jnp.arange(quarter * 2, dtype=jnp.int32) // 2
    outgoing = (
        jnp.zeros((seq_devices * capacity, D), jnp.bfloat16).at[own_slots].set(own_rows[token_of])
    )
    received = lax.all_to_all(
        outgoing.reshape(seq_devices, capacity, D), "sp", split_axis=0, concat_axis=0, tiled=True
    )
    gathered = lax.all_gather(received[:, None], "tp", axis=1, tiled=True)
    expert_in = gathered.reshape(-1, D)
    gate_part = jnp.dot(expert_in, w_gate[0], preferred_element_type=jnp.float32)
    up_part = jnp.dot(expert_in, w_up[0], preferred_element_type=jnp.float32)
    hidden = (jax.nn.silu(gate_part) * up_part).astype(jnp.bfloat16)
    partial_value = jnp.dot(hidden, w_down[0], preferred_element_type=jnp.float32)
    columns = lax.psum_scatter(
        partial_value.astype(jnp.bfloat16), "tp", scatter_dimension=1, tiled=True
    )
    col_count = columns.shape[1]
    returned = lax.all_to_all(
        columns.reshape(seq_devices, tp_devices * capacity, col_count),
        "sp",
        split_axis=0,
        concat_axis=0,
        tiled=True,
    )
    lookup = returned.reshape(-1, col_count)
    col_count = lookup.shape[1]
    picked = lookup[slots].reshape(row_count, 2, col_count).astype(jnp.float32)
    first_gate = group_weight * jax.nn.sigmoid(score_gap)
    second_gate = group_weight * jax.nn.sigmoid(-score_gap)
    result = middle_wide + first_gate[:, None] * picked[:, 0] + second_gate[:, None] * picked[:, 1]
    return result.astype(jnp.bfloat16)


def solution(mesh):
    return jax.shard_map(
        shards,
        mesh=mesh,
        in_specs=(
            P("sp", "tp"),
            P("sp", "tp"),
            P(None, "tp"),
            P("tp"),
            P("tp"),
            P("tp", None),
            P("sp", "tp"),
            P("tp"),
            P("sp", None),
            P("sp"),
            P("sp"),
            P("sp", None, "tp"),
            P("sp", None, "tp"),
            P("sp", "tp", None),
        ),
        out_specs=P("sp", "tp"),
        check_vma=False,
    )
```

profile of v0, /device:TPU:0, one launch (start us, length us, event | category | flops | bytes accessed | tf_op | source)
XLA Modules:
  0.0 363.9 jit_solution(2769100146873338767)
XLA Ops:
  6.5 0.8 slice.205
  7.4 4.9 %collective-permute-start = (bf16[30,256]{1,0:T(8,128)(2,1)S(1)}, bf16[30,256]{1,0:T(8,128)(2,1)S(1)}, u32[]{:S(2)}, u32[]{:S(2)}) collective-permute-start(bf16[30,256]{1,0:T(8,128)(2,1)S(1)} %slice.205), channel_id=1, source_target_pairs={{0,4},{4,8},{8,12},{12,16},{16,20},{20,24},{24,28},{1,5},{5,9},{9,... | collective-permute-start | bytes 46088 | tf_op jit(solution)/shard_map/ppermute | solution.py:14
  12.2 0.7 slice.206
  12.9 3.4 collective-permute-start.1
  16.4 1.0 fusion.62
  17.4 1.0 fusion.63
  18.4 1.2 divide_multiply_fusion
  19.7 0.0 copy-start.8
  19.7 0.0 copy-start.11
  19.7 0.0 copy-start.12
  19.7 2.4 fusion.59
  22.1 6.1 %all-reduce = (f32[512]{0:T(512)S(1)}, f32[512]{0:T(512)S(1)}) all-reduce(f32[512]{0:T(512)S(1)} %get-tuple-element.6, f32[512]{0:T(512)S(1)} %get-tuple-element.5), channel_id=1, replica_groups=mesh['sp'=8,'tp'=4] {'tp'}, use_global_device_ids=true, to_apply=%region_3.0 | all-reduce | flops 1024 | bytes 8192 | tf_op jit(solution)/shard_map/psum | solution.py:46
  28.2 2.1 convolution_convert_fusion.1
  30.3 0.0 reduce-scatter.3.cloned.1.call-update
  30.3 0.7 copy-done.4
  31.0 0.1 copy.18
  31.2 0.2 eq.26
  31.3 2.3 reduce-window.6
  33.6 0.1 slice.307
  33.7 0.1 copy.20
  33.8 29.0 %reduce-scatter.3.cloned.1.call-done = bf16[512,512]{1,0:T(8,128)(2,1)} async-done(((bf16[512,2048]{1,0:T(8,128)(2,1)}), bf16[512,512]{1,0:T(8,128)(2,1)}) %reduce-scatter.3.cloned.1.call-update) | async-done | bytes 524304 | tf_op jit(solution)/shard_map/reduce_scatter | solution.py:54
  62.9 1.3 fusion.1
  64.1 5.8 %psum.23 = f32[512]{0:T(512)S(1)} all-reduce(f32[512]{0:T(512)S(1)} %fusion.1), channel_id=1, replica_groups=mesh['sp'=8,'tp'=4] {'tp'}, use_global_device_ids=true, to_apply=%region_9.10 | all-reduce | flops 512 | bytes 4096 | tf_op jit(solution)/shard_map/psum | solution.py:59
  69.9 2.0 fusion.3
  72.0 3.5 all-to-all-start
  75.4 0.0 all-gather.3.cloned.1.call-start
  75.5 0.2 reshape.168
  75.7 0.1 fusion.53
  75.8 8.4 %all-to-all-done = bf16[4,128,512]{2,1,0:T(8,128)(2,1)S(1)} async-done(((bf16[4,128,512]{2,1,0:T(8,128)(2,1)}), bf16[4,128,512]{2,1,0:T(8,128)(2,1)S(1)}, u32[]{:S(2)}, u32[]{:S(2)}) %all-to-all-start) | async-done | bytes 524320 | tf_op jit(solution)/shard_map/all_to_all | solution.py:71
  84.2 0.9 copy.28
  85.1 6.4 %scatter_custom_fusion = bf16[512,2048]{1,0:T(8,128)(2,1)S(1)} fusion(s32[256]{0:T(256)S(1)} %bitcast.130, bf16[128,2048]{1,0:T(8,128)(2,1)} %bitcast.93, s32[1024]{0:T(1024)S(1)} %pad_clamp_fusion, bf16[]{:T(256)} %constant.25.clone.1), kind=kCustom, calls=%fused_computation.23 | custom fusion | bytes 2097664 | tf_op jit(solution)/shard_map/scatter | solution.py:78
  91.4 53.6 %all_to_all.29 = bf16[8,64,2048]{2,1,0:T(8,128)(2,1)} all-to-all(bf16[8,64,2048]{2,1,0:T(8,128)(2,1)S(1)} %bitcast.90), channel_id=1, replica_groups=mesh['sp'=8,'tp'=4] {'sp'}, dimensions={0} | all-to-all | bytes 4194304 | tf_op jit(solution)/shard_map/all_to_all | solution.py:80
  145.1 0.0 all-gather.3.cloned.1.call-update
  145.1 0.2 reduce-scatter.5.cloned.1.call-start
  145.3 56.4 %all-gather.3.cloned.1.call-done = bf16[8,256,2048]{2,1,0:T(8,128)(2,1)} async-done(((bf16[8,64,2048]{2,1,0:T(8,128)(2,1)}), bf16[8,256,2048]{2,1,0:T(8,128)(2,1)}) %all-gather.3.cloned.1.call-update) | async-done | bytes 8388624 | tf_op jit(solution)/shard_map/all_gather | solution.py:83
  201.7 7.2 %fusion.11 = f32[2048,256]{1,0:T(8,128)} fusion(bf16[2048,2048]{1,0:T(8,128)(2,1)} %bitcast.131, bf16[1,2048,256]{2,1,0:T(8,128)(2,1)S(1)} %copy-done.9), kind=kOutput, calls=%fused_computation.21 | convolution fusion | flops 2147483648 | bytes 11534336 | tf_op jit(solution)/shard_map/dot_general | solution.py:85
  208.9 13.1 %convolution_convert_fusion = bf16[2048,2048]{1,0:T(8,128)(2,1)} fusion(bf16[2048,2048]{1,0:T(8,128)(2,1)} %bitcast.132, f32[2048,256]{1,0:T(8,128)} %fusion.11, bf16[1,256,2048]{2,1,0:T(8,128)(2,1)S(1)} %copy-done, bf16[1,2048,256]{2,1,0:T(8,128)(2,1)S(1)} %copy-done.10), kind=kOutput, calls=%fused_computation.3 | convolution fusion | flops 4302307328 | bytes 20971520 | tf_op jit(solution)/shard_map/dot_general | solution.py:88
  222.0 0.0 reduce-scatter.5.cloned.1.call-update
  222.0 71.4 %reduce-scatter.5.cloned.1.call-done = bf16[2048,512]{1,0:T(8,128)(2,1)} async-done(((bf16[2048,2048]{1,0:T(8,128)(2,1)}), bf16[2048,512]{1,0:T(8,128)(2,1)}) %reduce-scatter.5.cloned.1.call-update) | async-done | bytes 2097168 | tf_op jit(solution)/shard_map/reduce_scatter | solution.py:89
  293.4 5.6 %all-to-all-start.2 = ((bf16[8,256,512]{2,1,0:T(8,128)(2,1)}), bf16[8,256,512]{2,1,0:T(8,128)(2,1)S(1)}, u32[]{:S(2)}, u32[]{:S(2)}) async-start(bf16[8,256,512]{2,1,0:T(8,128)(2,1)} %bitcast.91), calls=%async_computation.4 | async-start | bytes 4194304 | tf_op jit(solution)/shard_map/all_to_all | solution.py:93
  299.1 0.1 copy.23
  299.2 0.2 mul.551
  299.5 47.6 %all-to-all-done.2 = bf16[8,256,512]{2,1,0:T(8,128)(2,1)S(1)} async-done(((bf16[8,256,512]{2,1,0:T(8,128)(2,1)}), bf16[8,256,512]{2,1,0:T(8,128)(2,1)S(1)}, u32[]{:S(2)}, u32[]{:S(2)}) %all-to-all-start.2) | async-done | bytes 2097184 | tf_op jit(solution)/shard_map/all_to_all | solution.py:93
  347.2 5.0 %gather_fusion = bf16[1024,512]{1,0:T(8,128)(2,1)} fusion(bf16[2048,512]{1,0:T(8,128)(2,1)S(1)} %bitcast.89, s32[1024]{0:T(1024)S(1)} %broadcast_clamp_fusion), kind=kCustom, calls=%fused_computation.1 | custom fusion | bytes 2101248 | tf_op jit(solution)/shard_map/gather | solution.py:102
  352.2 2.4 reshape.174
  354.6 0.0 copy-start.2
  354.6 1.6 fusion.61
  356.3 1.1 fusion.5
  (40 shorter events, 0.2 us)
Async XLA Ops:
  6.5 202.4 %copy-start = (bf16[1,256,2048]{2,1,0:T(8,128)(2,1)S(1)}, bf16[1,256,2048]{2,1,0:T(8,128)(2,1)}, u32[]{:S(2)}) copy-start(bf16[1,256,2048]{2,1,0:T(8,128)(2,1)} %param.27) | copy-start | bytes 3145732
  6.5 56.3 %reduce-scatter.3.cloned.1.call-start = ((), (), s32[]{:S(2)}) async-start(), calls=%async_computation.5 | async-start | bytes 2621440 | tf_op jit(solution)/shard_map/reduce_scatter | solution.py:54
  7.4 11.1 %collective-permute-start = (bf16[30,256]{1,0:T(8,128)(2,1)S(1)}, bf16[30,256]{1,0:T(8,128)(2,1)S(1)}, u32[]{:S(2)}, u32[]{:S(2)}) collective-permute-start(bf16[30,256]{1,0:T(8,128)(2,1)S(1)} %slice.205), channel_id=1, source_target_pairs={{0,4},{4,8},{8,12},{12,16},{16,20},{20,24},{24,28},{1,5},{5,9},{9,... | collective-permute-start | bytes 46088 | tf_op jit(solution)/shard_map/ppermute | solution.py:14
  12.9 5.5 %collective-permute-start.1 = (bf16[30,256]{1,0:T(8,128)(2,1)S(1)}, bf16[30,256]{1,0:T(8,128)(2,1)S(1)}, u32[]{:S(2)}, u32[]{:S(2)}) collective-permute-start(bf16[30,256]{1,0:T(8,128)(2,1)S(1)} %slice.206), channel_id=1, source_target_pairs={{0,4},{4,8},{8,12},{12,16},{16,20},{20,24},{24,28},{1,5},{5,9},{9,... | collective-permute-start | bytes 46088 | tf_op jit(solution)/shard_map/ppermute | solution.py:14
  19.7 8.5 %copy-start.8 = (bf16[256,2048]{1,0:T(8,128)(2,1)S(1)}, bf16[256,2048]{1,0:T(8,128)(2,1)}, u32[]{:S(2)}) copy-start(bf16[256,2048]{1,0:T(8,128)(2,1)} %param.19) | copy-start | bytes 3145732
  19.7 8.5 %copy-start.11 = (f32[256]{0:T(256)S(1)}, f32[256]{0:T(256)}, u32[]{:S(2)}) copy-start(f32[256]{0:T(256)} %param.18) | copy-start | bytes 3076
  19.7 8.5 %copy-start.12 = (f32[256]{0:T(256)S(1)}, f32[256]{0:T(256)}, u32[]{:S(2)}) copy-start(f32[256]{0:T(256)} %param.17) | copy-start | bytes 3076
  30.3 0.7 copy-start.4
  30.3 32.5 %copy-start.1 = (bf16[512,512]{1,0:T(8,128)(2,1)S(1)}, bf16[512,512]{1,0:T(8,128)(2,1)}, u32[]{:S(2)}) copy-start(bf16[512,512]{1,0:T(8,128)(2,1)} %param.20) | copy-start | bytes 1572868
  30.3 39.6 %copy-start.5 = (f32[512]{0:T(512)S(1)}, f32[512]{0:T(512)}, u32[]{:S(2)}) copy-start(f32[512]{0:T(512)} %param.21) | copy-start | bytes 6148
  72.0 12.3 %all-to-all-start = ((bf16[4,128,512]{2,1,0:T(8,128)(2,1)}), bf16[4,128,512]{2,1,0:T(8,128)(2,1)S(1)}, u32[]{:S(2)}, u32[]{:S(2)}) async-start(bf16[4,128,512]{2,1,0:T(8,128)(2,1)} %bitcast.36), calls=%async_computation.1 | async-start | bytes 1048576 | tf_op jit(solution)/shard_map/all_to_all | solution.py:71
  75.4 126.3 %all-gather.3.cloned.1.call-start = ((), (), s32[]{:S(2)}) async-start(), calls=%async_computation.7 | async-start | bytes 10485760 | tf_op jit(solution)/shard_map/all_gather | solution.py:83
  145.1 56.7 %copy-start.9 = (bf16[1,2048,256]{2,1,0:T(8,128)(2,1)S(1)}, bf16[1,2048,256]{2,1,0:T(8,128)(2,1)}, u32[]{:S(2)}) copy-start(bf16[1,2048,256]{2,1,0:T(8,128)(2,1)} %param.25) | copy-start | bytes 3145732
  145.1 148.3 %reduce-scatter.5.cloned.1.call-start = ((), (), s32[]{:S(2)}) async-start(), calls=%async_computation.6 | async-start | bytes 10485760 | tf_op jit(solution)/shard_map/reduce_scatter | solution.py:89
  201.7 7.2 %copy-start.10 = (bf16[1,2048,256]{2,1,0:T(8,128)(2,1)S(1)}, bf16[1,2048,256]{2,1,0:T(8,128)(2,1)}, u32[]{:S(2)}) copy-start(bf16[1,2048,256]{2,1,0:T(8,128)(2,1)} %param.26) | copy-start | bytes 3145732
  293.4 6.1 %copy-start.6 = (f32[512]{0:T(512)S(1)}, f32[512]{0:T(512)}, u32[]{:S(2)}) copy-start(f32[512]{0:T(512)} %param.23) | copy-start | bytes 6148
  293.4 6.1 %copy-start.7 = (f32[512]{0:T(512)S(1)}, f32[512]{0:T(512)}, u32[]{:S(2)}) copy-start(f32[512]{0:T(512)} %param.24) | copy-start | bytes 6148
  293.4 53.7 %all-to-all-start.2 = ((bf16[8,256,512]{2,1,0:T(8,128)(2,1)}), bf16[8,256,512]{2,1,0:T(8,128)(2,1)S(1)}, u32[]{:S(2)}, u32[]{:S(2)}) async-start(bf16[8,256,512]{2,1,0:T(8,128)(2,1)} %bitcast.91), calls=%async_computation.4 | async-start | bytes 4194304 | tf_op jit(solution)/shard_map/all_to_all | solution.py:93
  354.6 1.7 copy-start.2
  354.6 1.6 copy-start.3
Sparse Core Ops, SparseCore 0:
  30.5 32.3 reduce-scatter.2
  145.2 56.4 all-gather.2
  222.2 71.2 reduce-scatter.4
where the time goes:
time: 365 us; the launch traced here: 364 us
  waiting for transfers between devices  213 us (58%)
  blocking collectives  65.4 us (18%)
  matrix products  22.4 us (6%)
  local copies, waits for them, and re-layouts  21.5 us (6%)
  starting transfers between devices  17.7 us (5%)
  between operations  13.4 us (4%)
  other arithmetic  10.5 us (3%)
    reduce_scatter x1, waiting for transfers between devices, shards(): lax.psum_scatter(partial_value.astype(jnp.bfloat16), 'tp', scatter_dimens...  71.4 us
    all_gather x1, waiting for transfers between devices, shards(): gathered = lax.all_gather(received[:, None], 'tp', axis=1, tiled=True)  56.4 us
    all_to_all x1, blocking collectives, shards(): lax.all_to_all(outgoing.reshape(seq_devices, capacity, D), 'sp', split_ax...  53.6 us
    all_to_all x1, waiting for transfers between devices, shards(): lax.all_to_all(columns.reshape(seq_devices, tp_devices * capacity, col_co...  47.6 us
    reduce_scatter x1, waiting for transfers between devices, shards(): lax.psum_scatter(partial_out.astype(jnp.bfloat16), 'tp', scatter_dimensio...  29 us
    dot_general x1, matrix products, shards(): jnp.dot(hidden, w_down[0], preferred_element_type=jnp.float32)  13.1 us
    all_to_all x1, waiting for transfers between devices, shards(): lax.all_to_all(normed, 'tp', split_axis=0, concat_axis=1, tiled=True)  8.4 us
    ppermute x2, starting transfers between devices, passed_along(): lax.ppermute(value, axis, [(source, source + steps) for source in range(l...  8.3 us
  transfers between devices with their start and end apart: 7, of which 5 were waited for; matrix products, arithmetic and copies ran while one was open for 2% of the time, Pallas kernels for 0%

commit v1 on v0

--- a/solution.py
+++ b/solution.py
@@ -80,7 +80,7 @@
     received = lax.all_to_all(
         outgoing.reshape(seq_devices, capacity, D), "sp", split_axis=0, concat_axis=0, tiled=True
     )
-    gathered = lax.all_gather(received[:, None], "tp", axis=1, tiled=True)
+    gathered = jnp.concatenate(lax.all_gather(received[:, None], "tp"), axis=1)
     expert_in = gathered.reshape(-1, D)
     gate_part = jnp.dot(expert_in, w_gate[0], preferred_element_type=jnp.float32)
     up_part = jnp.dot(expert_in, w_up[0], preferred_element_type=jnp.float32)

time: 365 us -> 373 us (1.022)
  local copies, waits for them, and re-layouts: 21.5 us -> 29.9 us
    reshape x0 -> x1, local copies, waits for them, and re-layouts: none -> 8.35 us  [shards(): gathered = jnp.concatenate(lax.all_gather(received[:, None], 'tp'), axis=1)]
where the time goes in v1:
time: 373 us; the launch traced here: 372 us
  waiting for transfers between devices  213 us (57%)
  blocking collectives  65.4 us (18%)
  local copies, waits for them, and re-layouts  29.9 us (8%)
  matrix products  22.4 us (6%)
  starting transfers between devices  17.7 us (5%)
  between operations  13.4 us (4%)
  other arithmetic  10.5 us (3%)
    reduce_scatter x1, waiting for transfers between devices, shards(): lax.psum_scatter(partial_value.astype(jnp.bfloat16), 'tp', scatter_dimens...  71.4 us
    all_gather x1, waiting for transfers between devices, shards(): gathered = jnp.concatenate(lax.all_gather(received[:, None], 'tp'), axis=1)  56.4 us
    all_to_all x1, blocking collectives, shards(): lax.all_to_all(outgoing.reshape(seq_devices, capacity, D), 'sp', split_ax...  53.6 us
    all_to_all x1, waiting for transfers between devices, shards(): lax.all_to_all(columns.reshape(seq_devices, tp_devices * capacity, col_co...  47.6 us
    reduce_scatter x1, waiting for transfers between devices, shards(): lax.psum_scatter(partial_out.astype(jnp.bfloat16), 'tp', scatter_dimensio...  29 us
    dot_general x1, matrix products, shards(): jnp.dot(hidden, w_down[0], preferred_element_type=jnp.float32)  13.1 us
    all_to_all x1, waiting for transfers between devices, shards(): lax.all_to_all(normed, 'tp', split_axis=0, concat_axis=1, tiled=True)  8.4 us
    reshape x1, local copies, waits for them, and re-layouts, shards(): gathered = jnp.concatenate(lax.all_gather(received[:, None], 'tp'), axis=1)  8.35 us
  transfers between devices with their start and end apart: 7, of which 5 were waited for; matrix products, arithmetic and copies ran while one was open for 2% of the time, Pallas kernels for 0%

profile of v1, /device:TPU:0, one launch (start us, length us, event | category | flops | bytes accessed | tf_op | source)
XLA Modules:
  0.0 372.2 jit_solution(5035283773459256999)
XLA Ops:
  6.5 0.8 slice.205
  7.4 4.9 %collective-permute-start = (bf16[30,256]{1,0:T(8,128)(2,1)S(1)}, bf16[30,256]{1,0:T(8,128)(2,1)S(1)}, u32[]{:S(2)}, u32[]{:S(2)}) collective-permute-start(bf16[30,256]{1,0:T(8,128)(2,1)S(1)} %slice.205), channel_id=1, source_target_pairs={{0,4},{4,8},{8,12},{12,16},{16,20},{20,24},{24,28},{1,5},{5,9},{9,... | collective-permute-start | bytes 46088 | tf_op jit(solution)/shard_map/ppermute | solution.py:14
  12.2 0.7 slice.206
  12.9 3.4 collective-permute-start.1
  16.4 1.0 fusion.62
  17.4 1.0 fusion.63
  18.4 1.2 divide_multiply_fusion
  19.7 0.0 copy-start.8
  19.7 0.0 copy-start.11
  19.7 2.4 fusion.59
  22.1 6.1 %all-reduce = (f32[512]{0:T(512)S(1)}, f32[512]{0:T(512)S(1)}) all-reduce(f32[512]{0:T(512)S(1)} %get-tuple-element.6, f32[512]{0:T(512)S(1)} %get-tuple-element.5), channel_id=1, replica_groups=mesh['sp'=8,'tp'=4] {'tp'}, use_global_device_ids=true, to_apply=%region_3.0 | all-reduce | flops 1024 | bytes 8192 | tf_op jit(solution)/shard_map/psum | solution.py:46
  28.2 2.1 convolution_convert_fusion.1
  30.3 0.0 reduce-scatter.3.cloned.1.call-update
  30.3 0.7 copy-done.4
  31.0 0.1 copy.35
  31.2 0.2 eq.26
  31.3 2.3 reduce-window.6
  33.6 0.1 slice.307
  33.7 0.1 copy.37
  33.8 29.0 %reduce-scatter.3.cloned.1.call-done = bf16[512,512]{1,0:T(8,128)(2,1)} async-done(((bf16[512,2048]{1,0:T(8,128)(2,1)}), bf16[512,512]{1,0:T(8,128)(2,1)}) %reduce-scatter.3.cloned.1.call-update) | async-done | bytes 524304 | tf_op jit(solution)/shard_map/reduce_scatter | solution.py:54
  62.9 1.3 fusion.1
  64.1 5.8 %psum.23 = f32[512]{0:T(512)S(1)} all-reduce(f32[512]{0:T(512)S(1)} %fusion.1), channel_id=1, replica_groups=mesh['sp'=8,'tp'=4] {'tp'}, use_global_device_ids=true, to_apply=%region_9.10 | all-reduce | flops 512 | bytes 4096 | tf_op jit(solution)/shard_map/psum | solution.py:59
  69.9 2.0 fusion.3
  72.0 3.5 all-to-all-start
  75.4 0.0 all-gather.3.cloned.1.call-start
  75.5 0.2 reshape.168
  75.7 0.1 fusion.53
  75.8 8.4 %all-to-all-done = bf16[4,128,512]{2,1,0:T(8,128)(2,1)S(1)} async-done(((bf16[4,128,512]{2,1,0:T(8,128)(2,1)}), bf16[4,128,512]{2,1,0:T(8,128)(2,1)S(1)}, u32[]{:S(2)}, u32[]{:S(2)}) %all-to-all-start) | async-done | bytes 524320 | tf_op jit(solution)/shard_map/all_to_all | solution.py:71
  84.2 0.9 copy.46
  85.1 6.4 %scatter_custom_fusion = bf16[512,2048]{1,0:T(8,128)(2,1)S(1)} fusion(s32[256]{0:T(256)S(1)} %bitcast.136, bf16[128,2048]{1,0:T(8,128)(2,1)} %bitcast.99, s32[1024]{0:T(1024)S(1)} %pad_clamp_fusion, bf16[]{:T(256)} %constant.25.clone.1), kind=kCustom, calls=%fused_computation.23 | custom fusion | bytes 2097664 | tf_op jit(solution)/shard_map/scatter | solution.py:78
  91.4 53.6 %all_to_all.29 = bf16[8,64,2048]{2,1,0:T(8,128)(2,1)} all-to-all(bf16[8,64,2048]{2,1,0:T(8,128)(2,1)S(1)} %bitcast.96), channel_id=1, replica_groups=mesh['sp'=8,'tp'=4] {'sp'}, dimensions={0} | all-to-all | bytes 4194304 | tf_op jit(solution)/shard_map/all_to_all | solution.py:80
  145.1 0.0 all-gather.3.cloned.1.call-update
  145.1 0.2 reduce-scatter.5.cloned.1.call-start
  145.3 56.4 %all-gather.3.cloned.1.call-done = bf16[32,64,2048]{2,1,0:T(8,128)(2,1)} async-done(((bf16[8,64,2048]{2,1,0:T(8,128)(2,1)}), bf16[32,64,2048]{2,1,0:T(8,128)(2,1)}) %all-gather.3.cloned.1.call-update) | async-done | bytes 8388624 | tf_op jit(solution)/shard_map/all_gather | solution.py:83
  201.7 8.4 %copy.40 = bf16[8,4,1,64,2048]{4,3,1,0,2:T(8,128)(2,1)} copy(bf16[8,4,1,64,2048]{4,3,0,1,2:T(8,128)(2,1)} %bitcast.93) | data formatting | bytes 16777216 | tf_op jit(solution)/shard_map/reshape | solution.py:83
  210.1 7.2 %fusion.11 = f32[2048,256]{1,0:T(8,128)} fusion(bf16[2048,2048]{1,0:T(8,128)(2,1)} %bitcast.94, bf16[1,2048,256]{2,1,0:T(8,128)(2,1)S(1)} %copy-done.9), kind=kOutput, calls=%fused_computation.21 | convolution fusion | flops 2147483648 | bytes 11534336 | tf_op jit(solution)/shard_map/dot_general | solution.py:85
  217.3 13.1 %convolution_convert_fusion = bf16[2048,2048]{1,0:T(8,128)(2,1)} fusion(bf16[2048,2048]{1,0:T(8,128)(2,1)} %bitcast.95, f32[2048,256]{1,0:T(8,128)} %fusion.11, bf16[1,256,2048]{2,1,0:T(8,128)(2,1)S(1)} %copy-done, bf16[1,2048,256]{2,1,0:T(8,128)(2,1)S(1)} %copy-done.10), kind=kOutput, calls=%fused_computation.3 | convolution fusion | flops 4302307328 | bytes 20971520 | tf_op jit(solution)/shard_map/dot_general | solution.py:88
  230.4 0.0 reduce-scatter.5.cloned.1.call-update
  230.4 71.4 %reduce-scatter.5.cloned.1.call-done = bf16[2048,512]{1,0:T(8,128)(2,1)} async-done(((bf16[2048,2048]{1,0:T(8,128)(2,1)}), bf16[2048,512]{1,0:T(8,128)(2,1)}) %reduce-scatter.5.cloned.1.call-update) | async-done | bytes 2097168 | tf_op jit(solution)/shard_map/reduce_scatter | solution.py:89
  301.8 5.6 %all-to-all-start.2 = ((bf16[8,256,512]{2,1,0:T(8,128)(2,1)}), bf16[8,256,512]{2,1,0:T(8,128)(2,1)S(1)}, u32[]{:S(2)}, u32[]{:S(2)}) async-start(bf16[8,256,512]{2,1,0:T(8,128)(2,1)} %bitcast.97), calls=%async_computation.4 | async-start | bytes 4194304 | tf_op jit(solution)/shard_map/all_to_all | solution.py:93
  307.5 0.1 copy.41
  307.6 0.2 mul.551
  307.9 47.6 %all-to-all-done.2 = bf16[8,256,512]{2,1,0:T(8,128)(2,1)S(1)} async-done(((bf16[8,256,512]{2,1,0:T(8,128)(2,1)}), bf16[8,256,512]{2,1,0:T(8,128)(2,1)S(1)}, u32[]{:S(2)}, u32[]{:S(2)}) %all-to-all-start.2) | async-done | bytes 2097184 | tf_op jit(solution)/shard_map/all_to_all | solution.py:93
  355.5 5.0 %gather_fusion = bf16[1024,512]{1,0:T(8,128)(2,1)} fusion(bf16[2048,512]{1,0:T(8,128)(2,1)S(1)} %bitcast.92, s32[1024]{0:T(1024)S(1)} %broadcast_clamp_fusion), kind=kCustom, calls=%fused_computation.1 | custom fusion | bytes 2101248 | tf_op jit(solution)/shard_map/gather | solution.py:102
  360.6 2.4 reshape.174
  363.0 0.0 copy-start.2
  363.0 1.6 fusion.61
  364.6 1.1 fusion.5
  (41 shorter events, 0.2 us)
Async XLA Ops:
  6.5 210.7 %copy-start = (bf16[1,256,2048]{2,1,0:T(8,128)(2,1)S(1)}, bf16[1,256,2048]{2,1,0:T(8,128)(2,1)}, u32[]{:S(2)}) copy-start(bf16[1,256,2048]{2,1,0:T(8,128)(2,1)} %param.27) | copy-start | bytes 3145732
  6.5 56.3 %reduce-scatter.3.cloned.1.call-start = ((), (), s32[]{:S(2)}) async-start(), calls=%async_computation.5 | async-start | bytes 2621440 | tf_op jit(solution)/shard_map/reduce_scatter | solution.py:54
  7.4 11.1 %collective-permute-start = (bf16[30,256]{1,0:T(8,128)(2,1)S(1)}, bf16[30,256]{1,0:T(8,128)(2,1)S(1)}, u32[]{:S(2)}, u32[]{:S(2)}) collective-permute-start(bf16[30,256]{1,0:T(8,128)(2,1)S(1)} %slice.205), channel_id=1, source_target_pairs={{0,4},{4,8},{8,12},{12,16},{16,20},{20,24},{24,28},{1,5},{5,9},{9,... | collective-permute-start | bytes 46088 | tf_op jit(solution)/shard_map/ppermute | solution.py:14
  12.9 5.5 %collective-permute-start.1 = (bf16[30,256]{1,0:T(8,128)(2,1)S(1)}, bf16[30,256]{1,0:T(8,128)(2,1)S(1)}, u32[]{:S(2)}, u32[]{:S(2)}) collective-permute-start(bf16[30,256]{1,0:T(8,128)(2,1)S(1)} %slice.206), channel_id=1, source_target_pairs={{0,4},{4,8},{8,12},{12,16},{16,20},{20,24},{24,28},{1,5},{5,9},{9,... | collective-permute-start | bytes 46088 | tf_op jit(solution)/shard_map/ppermute | solution.py:14
  19.7 8.5 %copy-start.8 = (bf16[256,2048]{1,0:T(8,128)(2,1)S(1)}, bf16[256,2048]{1,0:T(8,128)(2,1)}, u32[]{:S(2)}) copy-start(bf16[256,2048]{1,0:T(8,128)(2,1)} %param.19) | copy-start | bytes 3145732
  19.7 8.5 %copy-start.11 = (f32[256]{0:T(256)S(1)}, f32[256]{0:T(256)}, u32[]{:S(2)}) copy-start(f32[256]{0:T(256)} %param.18) | copy-start | bytes 3076
  19.7 8.5 %copy-start.12 = (f32[256]{0:T(256)S(1)}, f32[256]{0:T(256)}, u32[]{:S(2)}) copy-start(f32[256]{0:T(256)} %param.17) | copy-start | bytes 3076
  30.3 0.7 copy-start.4
  30.3 32.5 %copy-start.1 = (bf16[512,512]{1,0:T(8,128)(2,1)S(1)}, bf16[512,512]{1,0:T(8,128)(2,1)}, u32[]{:S(2)}) copy-start(bf16[512,512]{1,0:T(8,128)(2,1)} %param.20) | copy-start | bytes 1572868
  30.3 39.6 %copy-start.5 = (f32[512]{0:T(512)S(1)}, f32[512]{0:T(512)}, u32[]{:S(2)}) copy-start(f32[512]{0:T(512)} %param.21) | copy-start | bytes 6148
  72.0 12.3 %all-to-all-start = ((bf16[4,128,512]{2,1,0:T(8,128)(2,1)}), bf16[4,128,512]{2,1,0:T(8,128)(2,1)S(1)}, u32[]{:S(2)}, u32[]{:S(2)}) async-start(bf16[4,128,512]{2,1,0:T(8,128)(2,1)} %bitcast.36), calls=%async_computation.1 | async-start | bytes 1048576 | tf_op jit(solution)/shard_map/all_to_all | solution.py:71
  75.4 126.3 %all-gather.3.cloned.1.call-start = ((), (), s32[]{:S(2)}) async-start(), calls=%async_computation.7 | async-start | bytes 10485760 | tf_op jit(solution)/shard_map/all_gather | solution.py:83
  145.1 156.7 %reduce-scatter.5.cloned.1.call-start = ((), (), s32[]{:S(2)}) async-start(), calls=%async_computation.6 | async-start | bytes 10485760 | tf_op jit(solution)/shard_map/reduce_scatter | solution.py:89
  201.7 8.4 %copy-start.9 = (bf16[1,2048,256]{2,1,0:T(8,128)(2,1)S(1)}, bf16[1,2048,256]{2,1,0:T(8,128)(2,1)}, u32[]{:S(2)}) copy-start(bf16[1,2048,256]{2,1,0:T(8,128)(2,1)} %param.25) | copy-start | bytes 3145732
  210.1 7.2 %copy-start.10 = (bf16[1,2048,256]{2,1,0:T(8,128)(2,1)S(1)}, bf16[1,2048,256]{2,1,0:T(8,128)(2,1)}, u32[]{:S(2)}) copy-start(bf16[1,2048,256]{2,1,0:T(8,128)(2,1)} %param.26) | copy-start | bytes 3145732
  301.8 6.1 %copy-start.6 = (f32[512]{0:T(512)S(1)}, f32[512]{0:T(512)}, u32[]{:S(2)}) copy-start(f32[512]{0:T(512)} %param.23) | copy-start | bytes 6148
  301.8 6.1 %copy-start.7 = (f32[512]{0:T(512)S(1)}, f32[512]{0:T(512)}, u32[]{:S(2)}) copy-start(f32[512]{0:T(512)} %param.24) | copy-start | bytes 6148
  301.8 53.7 %all-to-all-start.2 = ((bf16[8,256,512]{2,1,0:T(8,128)(2,1)}), bf16[8,256,512]{2,1,0:T(8,128)(2,1)S(1)}, u32[]{:S(2)}, u32[]{:S(2)}) async-start(bf16[8,256,512]{2,1,0:T(8,128)(2,1)} %bitcast.97), calls=%async_computation.4 | async-start | bytes 4194304 | tf_op jit(solution)/shard_map/all_to_all | solution.py:93
  363.0 1.7 copy-start.2
  363.0 1.6 copy-start.3
Sparse Core Ops, SparseCore 0:
  30.5 32.3 reduce-scatter.2
  145.2 56.4 all-gather.2
  230.5 71.2 reduce-scatter.4
